TPU v7x, 32 devices: a whole 2x2x4 slice. The times are simulated.
32 devices in a mesh: sp: 4 (over z), dp: 8 (over y, x, core).
Axes of the slice: x: 2, y: 2, z: 4, core: 2. Of those that a mesh axis runs over, the one named last changes fastest.
Arguments:
- value_half: bfloat16 [8, 1536, 2048], P('dp', 'sp'), may hold values from -6 to 6
- gate_half: bfloat16 [8, 1536, 2048], P('dp', 'sp'), may hold values from -9 to 9
- conv_taps: bfloat16 [31, 2048], replicated, may hold values from -1 to 1
- norm_gain: float32 [2048], replicated, may hold values from 0.1 to 1.9
- norm_shift: float32 [2048], replicated, may hold values from -3 to 3
- out_weight: bfloat16 [2048, 2048], P('dp', 'sp'), may hold values from -0.125 to 0.125
Outputs:
- module_out: bfloat16 [8, 1536, 2048], P('dp', 'sp')
All inputs are finite; a program needn't handle non-finite values.
Results may differ from a plain program's by a relative error of at most 0.0064.
Values may be sent and summed in bfloat16 or wider, within the bound.
A program may use at most 64 MiB of HBM per device.

v0:
```python
import jax
import jax.numpy as jnp
from jax import lax
from jax.sharding import PartitionSpec as P

EPSILON = 1e-06


def passed_along(value, axis, steps):
    count = lax.axis_size(axis)
    initial, last = (max(0, -steps), min(count, count - steps))
    return lax.ppermute(value, axis, [(source, source + steps) for source in range(initial, last)])


def causal_mix(padded, conv_taps, length):
    tap_count = conv_taps.shape[0]
    running = jnp.zeros((length, padded.shape[1]), jnp.float32)
    for tap_index in range(tap_count):
        running = running + padded[tap_index : tap_index + length].astype(jnp.float32) * conv_taps[
            tap_index
        ].astype(jnp.float32)
    return running.astype(jnp.bfloat16)


def per_device(value_half, gate_half, conv_taps, norm_gain, norm_shift, out_weight):
    tap_count = conv_taps.shape[0]
    tok_rows = value_half.shape[1]
    gated = (
        value_half[0].astype(jnp.float32) * jax.nn.sigmoid(gate_half[0].astype(jnp.float32))
    ).astype(jnp.bfloat16)
    tail_rows = gated[tok_rows - (tap_count - 1) :]
    history = passed_along(tail_rows, "sp", 1)
    padded = jnp.concatenate([history, gated], 0)
    convolved = causal_mix(padded, conv_taps, tok_rows)
    widened = convolved.astype(jnp.float32)
    mean_row = jnp.mean(widened, axis=-1, keepdims=True)
    centered = widened - mean_row
    variance = jnp.mean(centered * centered, axis=-1, keepdims=True)
    normed = centered * lax.rsqrt(variance + EPSILON) * norm_gain + norm_shift
    activated = jax.nn.silu(normed).astype(jnp.bfloat16)
    row_block = lax.all_gather(out_weight, "sp", axis=1, tiled=True)
    projected = jnp.dot(
        activated,
        lax.all_gather(row_block, "dp", axis=0, tiled=True),
        preferred_element_type=jnp.float32,
    )
    return projected.astype(jnp.bfloat16)[None]


def solution(mesh):
    placed = (P("dp", "sp", None), P("dp", "sp", None), P(), P(), P(), P("dp", "sp"))
    return jax.shard_map(
        per_device, mesh=mesh, in_specs=placed, out_specs=P("dp", "sp", None), check_vma=False
    )
```

profile of v0, /device:TPU:0, one launch (start us, length us, event | category | flops | bytes accessed | tf_op | source)
XLA Modules:
  0.0 110.5 jit_solution(4330929815768049006)
XLA Ops:
  6.5 0.0 copy-start
  6.5 0.0 all-gather.3.cloned.1.call-start
  6.5 0.7 all-gather.3.cloned.1.call-update
  7.3 0.0 all-gather.5.cloned.1.call-start
  7.3 32.3 %all-gather.3.cloned.1.call-done = bf16[256,2048]{1,0:T(8,128)(2,1)} async-done(((bf16[256,512]{1,0:T(8,128)(2,1)}), bf16[256,2048]{1,0:T(8,128)(2,1)}) %all-gather.3.cloned.1.call-update) | async-done | bytes 1048592 | tf_op jit(solution)/shard_map/all_gather | solution.py:41
  39.6 0.0 all-gather.5.cloned.1.call-update
  39.7 2.8 %multiply_convert_fusion = bf16[1,384,2048]{2,1,0:T(8,128)(2,1)S(1)} fusion(bf16[1,384,2048]{2,1,0:T(8,128)(2,1)} %param.6, bf16[1,384,2048]{2,1,0:T(8,128)(2,1)} %param.7), kind=kLoop, calls=%fused_computation.42 | loop fusion | flops 5505024 | bytes 4718592 | tf_op jit(solution)/shard_map/convert_element_type | solution.py:30
  42.5 0.0 copy-start.1
  42.5 0.0 copy-start.2
  42.5 3.4 %collective-permute-start = (bf16[30,2048]{1,0:T(8,128)(2,1)S(1)}, bf16[30,2048]{1,0:T(8,128)(2,1)S(1)}, u32[]{:S(2)}, u32[]{:S(2)}) collective-permute-start(bf16[30,2048]{1,0:T(8,128)(2,1)S(1)} %slice_bitcast_fusion), channel_id=1, source_target_pairs={{0,8},{8,16},{16,24},{1,9},{9,17},{17,25},{2,10},{10,18},{18,26},{... | collective-permute-start | bytes 368648 | tf_op jit(solution)/shard_map/ppermute | solution.py:12
  45.9 0.0 copy-done
  45.9 0.1 slice_convert_fusion.30
  46.0 0.1 slice_convert_fusion.29
  46.1 2.3 %collective-permute-done = bf16[30,2048]{1,0:T(8,128)(2,1)S(1)} collective-permute-done((bf16[30,2048]{1,0:T(8,128)(2,1)S(1)}, bf16[30,2048]{1,0:T(8,128)(2,1)S(1)}, u32[]{:S(2)}, u32[]{:S(2)}) %collective-permute-start) | collective-permute-done | bytes 122912 | tf_op jit(solution)/shard_map/ppermute | solution.py:12
  48.4 14.3 %convert_reduce_fusion = (f32[384]{0:T(512)S(1)}, bf16[384,2048]{1,0:T(8,128)(2,1)S(1)}) fusion(f32[2048]{0:T(1024)S(1)} %bitcast.67, bf16[384,2048]{1,0:T(8,128)(2,1)S(1)} %bitcast.37, f32[2048]{0:T(1024)S(1)} %bitcast.68, bf16[30,2048]{1,0:T(8,128)(2,1)S(1)} %collective-permute-done, f32[2048]{0:T(1024)S(1)} %bitcast.39, f32[2048]{0:T(1024)S(1)} %bitcast.40, ...), kind=kLoop, calls=%fused_computation.30 | loop fusion | flops 145489536 | bytes 3524096 | tf_op jit(solution)/shard_map/reduce_sum | solution.py:36
  62.7 0.6 fusion.2
  63.2 31.9 %all-gather.5.cloned.1.call-done = bf16[2048,2048]{1,0:T(8,128)(2,1)} async-done(((bf16[256,2048]{1,0:T(8,128)(2,1)}), bf16[2048,2048]{1,0:T(8,128)(2,1)}) %all-gather.5.cloned.1.call-update) | async-done | bytes 8388624 | tf_op jit(solution)/shard_map/all_gather | solution.py:44
  95.2 0.0 copy-done.1
  95.2 0.0 copy-done.2
  95.2 8.5 %fusion.11 = bf16[1,384,2048]{2,1,0:T(8,128)(2,1)} fusion(bf16[2048,2048]{1,0:T(8,128)(2,1)} %all-gather.5.cloned.1.call-done, bf16[384,2048]{1,0:T(8,128)(2,1)S(1)} %get-tuple-element.6, f32[2048]{0:T(1024)S(1)} %copy-done.1, f32[2048]{0:T(1024)S(1)} %copy-done.2, f32[384]{0:T(512)S(1)} %add_rsqrt_fusion, f32[384]{0:T(512)S(1)} %broadcast_multiply_fusion), kind=kOutput, calls=%fused_computation.45 | convolution fusion | flops 3229876224 | bytes 11553792 | tf_op jit(solution)/shard_map/dot_general | solution.py:42
  (3 shorter events, 0.0 us)
Async XLA Ops:
  6.5 39.4 %copy-start = (bf16[31,2048]{1,0:T(8,128)(2,1)S(1)}, bf16[31,2048]{1,0:T(8,128)(2,1)}, u32[]{:S(2)}) copy-start(bf16[31,2048]{1,0:T(8,128)(2,1)} %param.8) | copy-start | bytes 380932
  6.5 33.1 %all-gather.3.cloned.1.call-start = ((), (), s32[]{:S(2)}) async-start(), calls=%async_computation | async-start | bytes 1310720 | tf_op jit(solution)/shard_map/all_gather | solution.py:41
  7.3 87.9 %all-gather.5.cloned.1.call-start = ((), (), s32[]{:S(2)}) async-start(), calls=%async_computation.1 | async-start | bytes 9437184 | tf_op jit(solution)/shard_map/all_gather | solution.py:44
  42.5 52.7 %copy-start.1 = (f32[2048]{0:T(1024)S(1)}, f32[2048]{0:T(1024)}, u32[]{:S(2)}) copy-start(f32[2048]{0:T(1024)} %param.10) | copy-start | bytes 24580
  42.5 52.7 %copy-start.2 = (f32[2048]{0:T(1024)S(1)}, f32[2048]{0:T(1024)}, u32[]{:S(2)}) copy-start(f32[2048]{0:T(1024)} %param.9) | copy-start | bytes 24580
  42.5 5.9 %collective-permute-start = (bf16[30,2048]{1,0:T(8,128)(2,1)S(1)}, bf16[30,2048]{1,0:T(8,128)(2,1)S(1)}, u32[]{:S(2)}, u32[]{:S(2)}) collective-permute-start(bf16[30,2048]{1,0:T(8,128)(2,1)S(1)} %slice_bitcast_fusion), channel_id=1, source_target_pairs={{0,8},{8,16},{16,24},{1,9},{9,17},{17,25},{2,10},{10,18},{18,26},{... | collective-permute-start | bytes 368648 | tf_op jit(solution)/shard_map/ppermute | solution.py:12
Sparse Core Ops, SparseCore 0:
  8.9 30.6 all-gather.2
  41.5 53.6 all-gather.4
where the time goes:
time: 111 us
  waiting for transfers between devices  67.3 us (61%)
  other arithmetic  17.8 us (16%)
  between operations  13.5 us (12%)
  matrix products  8.49 us (8%)
  starting transfers between devices  3.4 us (3%)
    all_gather x1, waiting for transfers between devices, per_device(): row_block = lax.all_gather(out_weight, 'sp', axis=1, tiled=True)  32.3 us
    all_gather x1, waiting for transfers between devices, per_device(): lax.all_gather(row_block, 'dp', axis=0, tiled=True)  31.9 us
    reduce_sum x1, other arithmetic, per_device(): mean_row = jnp.mean(widened, axis=-1, keepdims=True)  14.3 us
    dot_general x1, matrix products, per_device(): jnp.dot(activated, lax.all_gather(row_block, 'dp', axis=0, tiled=True), p...  8.49 us
    ppermute x1, starting transfers between devices, passed_along(): lax.ppermute(value, axis, [(source, source + steps) for source in range(i...  3.36 us
    convert_element_type x1, other arithmetic, per_device(): gated = (value_half[0].astype(jnp.float32) * jax.nn.sigmoid(gate_half[0]....  2.79 us
    ppermute x1, waiting for transfers between devices, passed_along(): lax.ppermute(value, axis, [(source, source + steps) for source in range(i...  2.29 us
  transfers between devices with their start and end apart: 3, of which 3 were waited for; matrix products, arithmetic and copies ran while one was open for 16% of the time, Pallas kernels for 0%

commit v1 on v0

--- a/solution.py
+++ b/solution.py
@@ -38,7 +38,8 @@
     variance = jnp.mean(centered * centered, axis=-1, keepdims=True)
     normed = centered * lax.rsqrt(variance + EPSILON) * norm_gain + norm_shift
     activated = jax.nn.silu(normed).astype(jnp.bfloat16)
-    row_block = lax.all_gather(out_weight, "sp", axis=1, tiled=True)
+    blocks = lax.all_gather(out_weight, "sp")
+    row_block = jnp.concatenate(blocks, axis=1)
     projected = jnp.dot(
         activated,
         lax.all_gather(row_block, "dp", axis=0, tiled=True),

time: 111 us -> 114 us (1.027)
  local copies, waits for them, and re-layouts: 0.05 us -> 2.31 us
  other arithmetic: 17.8 us -> 15.9 us
  waiting for transfers between devices: 67.3 us -> 69.1 us
  matrix products: 8.49 us -> 10.1 us
    reshape x0 -> x1, local copies, waits for them, and re-layouts: none -> 2.26 us  [per_device(): row_block = jnp.concatenate(blocks, axis=1)]
    convert_element_type x1, other arithmetic: 2.79 us -> 0.86 us  [per_device(): gated = (value_half[0].astype(jnp.float32) * jax.nn.sigmoid(gate_half[0]....]
    all_gather x1, waiting for transfers between devices: 31.9 us -> 33.7 us  [per_device(): lax.all_gather(row_block, 'dp', axis=0, tiled=True)]
    dot_general x1, matrix products: 8.49 us -> 10.1 us  [per_device(): jnp.dot(activated, lax.all_gather(row_block, 'dp', axis=0, tiled=True), p...]
  transfers between devices with their start and end apart: 3 -> 3, of which waited for: 3 -> 3; matrix products, arithmetic and copies ran while one was open for 16% -> 14% of each run, Pallas kernels for 0% -> 0%
where the time goes in v1:
time: 114 us
  waiting for transfers between devices  69.1 us (61%)
  other arithmetic  15.9 us (14%)
  between operations  13.5 us (12%)
  matrix products  10.1 us (9%)
  starting transfers between devices  3.4 us (3%)
  local copies, waits for them, and re-layouts  2.31 us (2%)
    all_gather x1, waiting for transfers between devices, per_device(): lax.all_gather(row_block, 'dp', axis=0, tiled=True)  33.7 us
    all_gather x1, waiting for transfers between devices, per_device(): blocks = lax.all_gather(out_weight, 'sp')  32.3 us
    reduce_sum x1, other arithmetic, per_device(): mean_row = jnp.mean(widened, axis=-1, keepdims=True)  14.3 us
    dot_general x1, matrix products, per_device(): jnp.dot(activated, lax.all_gather(row_block, 'dp', axis=0, tiled=True), p...  10.1 us
    ppermute x1, starting transfers between devices, passed_along(): lax.ppermute(value, axis, [(source, source + steps) for source in range(i...  3.36 us
    ppermute x1, waiting for transfers between devices, passed_along(): lax.ppermute(value, axis, [(source, source + steps) for source in range(i...  2.29 us
  transfers between devices with their start and end apart: 3, of which 3 were waited for; matrix products, arithmetic and copies ran while one was open for 14% of the time, Pallas kernels for 0%

profile of v1, /device:TPU:0, one launch (start us, length us, event | category | flops | bytes accessed | tf_op | source)
XLA Modules:
  0.0 114.3 jit_solution(8431388869520999883)
XLA Ops:
  6.5 0.0 copy-start
  6.5 0.0 copy-start.1
  6.5 0.0 all-gather.6.cloned.1.call-start
  6.5 0.7 all-gather.6.cloned.1.call-update
  7.3 0.0 all-gather.4.cloned.1.call-start
  7.3 32.3 %all-gather.6.cloned.1.call-done = bf16[1024,512]{1,0:T(8,128)(2,1)} async-done(((bf16[256,512]{1,0:T(8,128)(2,1)}), bf16[1024,512]{1,0:T(8,128)(2,1)}) %all-gather.6.cloned.1.call-update) | async-done | bytes 1048592 | tf_op jit(solution)/shard_map/all_gather | solution.py:41
  39.6 2.3 %copy.7 = bf16[256,4,512]{0,2,1:T(8,128)(2,1)} copy(bf16[256,4,512]{2,0,1:T(8,128)(2,1)} %bitcast.43) | data formatting | bytes 2097152 | tf_op jit(solution)/shard_map/reshape | solution.py:42
  41.9 0.0 copy-start.2
  41.9 0.0 all-gather.4.cloned.1.call-update
  41.9 0.0 copy-done
  41.9 0.0 copy-done.1
  41.9 0.9 multiply_convert_fusion
  42.8 0.0 copy-start.3
  42.8 0.0 copy-start.4
  42.9 3.4 %collective-permute-start = (bf16[30,2048]{1,0:T(8,128)(2,1)S(1)}, bf16[30,2048]{1,0:T(8,128)(2,1)S(1)}, u32[]{:S(2)}, u32[]{:S(2)}) collective-permute-start(bf16[30,2048]{1,0:T(8,128)(2,1)S(1)} %slice_bitcast_fusion), channel_id=1, source_target_pairs={{0,8},{8,16},{16,24},{1,9},{9,17},{17,25},{2,10},{10,18},{18,26},{... | collective-permute-start | bytes 368648 | tf_op jit(solution)/shard_map/ppermute | solution.py:12
  46.3 0.0 copy-done.2
  46.3 0.1 slice_convert_fusion.30
  46.4 0.1 slice_convert_fusion.29
  46.5 2.3 %collective-permute-done = bf16[30,2048]{1,0:T(8,128)(2,1)S(1)} collective-permute-done((bf16[30,2048]{1,0:T(8,128)(2,1)S(1)}, bf16[30,2048]{1,0:T(8,128)(2,1)S(1)}, u32[]{:S(2)}, u32[]{:S(2)}) %collective-permute-start) | collective-permute-done | bytes 122912 | tf_op jit(solution)/shard_map/ppermute | solution.py:12
  48.7 14.3 %convert_reduce_fusion = (f32[384]{0:T(512)S(1)}, bf16[384,2048]{1,0:T(8,128)(2,1)S(1)}) fusion(f32[2048]{0:T(1024)S(1)} %bitcast.73, bf16[384,2048]{1,0:T(8,128)(2,1)S(1)} %bitcast.41, f32[2048]{0:T(1024)S(1)} %bitcast.74, bf16[30,2048]{1,0:T(8,128)(2,1)S(1)} %collective-permute-done, f32[2048]{0:T(1024)S(1)} %bitcast.45, f32[2048]{0:T(1024)S(1)} %bitcast.46, ...), kind=kLoop, calls=%fused_computation.30 | loop fusion | flops 145489536 | bytes 3524096 | tf_op jit(solution)/shard_map/reduce_sum | solution.py:36
  63.0 0.6 fusion.2
  63.6 33.7 %all-gather.4.cloned.1.call-done = bf16[2048,2048]{0,1:T(8,128)(2,1)} async-done(((bf16[256,2048]{0,1:T(8,128)(2,1)}), bf16[2048,2048]{0,1:T(8,128)(2,1)}) %all-gather.4.cloned.1.call-update) | async-done | bytes 8388624 | tf_op jit(solution)/shard_map/all_gather | solution.py:45
  97.3 0.0 copy-done.3
  97.3 0.0 copy-done.4
  97.3 10.1 %fusion.11 = bf16[1,384,2048]{2,1,0:T(8,128)(2,1)} fusion(bf16[2048,2048]{0,1:T(8,128)(2,1)} %all-gather.4.cloned.1.call-done, bf16[384,2048]{1,0:T(8,128)(2,1)S(1)} %get-tuple-element.6, f32[2048]{0:T(1024)S(1)} %copy-done.3, f32[2048]{0:T(1024)S(1)} %copy-done.4, f32[384]{0:T(512)S(1)} %add_rsqrt_fusion, f32[384]{0:T(512)S(1)} %broadcast_multiply_fusion), kind=kOutput, calls=%fused_computation.45 | convolution fusion | flops 3229876224 | bytes 11553792 | tf_op jit(solution)/shard_map/dot_general | solution.py:43
  (3 shorter events, 0.0 us)
Async XLA Ops:
  6.5 35.4 %copy-start = (bf16[1,384,2048]{2,1,0:T(8,128)(2,1)S(1)}, bf16[1,384,2048]{2,1,0:T(8,128)(2,1)}, u32[]{:S(2)}) copy-start(bf16[1,384,2048]{2,1,0:T(8,128)(2,1)} %param.6) | copy-start | bytes 4718596
  6.5 35.4 %copy-start.1 = (bf16[1,384,2048]{2,1,0:T(8,128)(2,1)S(1)}, bf16[1,384,2048]{2,1,0:T(8,128)(2,1)}, u32[]{:S(2)}) copy-start(bf16[1,384,2048]{2,1,0:T(8,128)(2,1)} %param.7) | copy-start | bytes 4718596
  6.5 33.1 %all-gather.6.cloned.1.call-start = ((), (), s32[]{:S(2)}) async-start(), calls=%async_computation.1 | async-start | bytes 1310720 | tf_op jit(solution)/shard_map/all_gather | solution.py:41
  7.3 90.1 %all-gather.4.cloned.1.call-start = ((), (), s32[]{:S(2)}) async-start(), calls=%async_computation | async-start | bytes 9437184 | tf_op jit(solution)/shard_map/all_gather | solution.py:45
  41.9 4.4 %copy-start.2 = (bf16[31,2048]{1,0:T(8,128)(2,1)S(1)}, bf16[31,2048]{1,0:T(8,128)(2,1)}, u32[]{:S(2)}) copy-start(bf16[31,2048]{1,0:T(8,128)(2,1)} %param.8) | copy-start | bytes 380932
  42.8 54.5 %copy-start.3 = (f32[2048]{0:T(1024)S(1)}, f32[2048]{0:T(1024)}, u32[]{:S(2)}) copy-start(f32[2048]{0:T(1024)} %param.10) | copy-start | bytes 24580
  42.8 54.5 %copy-start.4 = (f32[2048]{0:T(1024)S(1)}, f32[2048]{0:T(1024)}, u32[]{:S(2)}) copy-start(f32[2048]{0:T(1024)} %param.9) | copy-start | bytes 24580
  42.9 5.9 %collective-permute-start = (bf16[30,2048]{1,0:T(8,128)(2,1)S(1)}, bf16[30,2048]{1,0:T(8,128)(2,1)S(1)}, u32[]{:S(2)}, u32[]{:S(2)}) collective-permute-start(bf16[30,2048]{1,0:T(8,128)(2,1)S(1)} %slice_bitcast_fusion), channel_id=1, source_target_pairs={{0,8},{8,16},{16,24},{1,9},{9,17},{17,25},{2,10},{10,18},{18,26},{... | collective-permute-start | bytes 368648 | tf_op jit(solution)/shard_map/ppermute | solution.py:12
Sparse Core Ops, SparseCore 0:
  8.9 30.6 all-gather.5
  42.0 55.2 all-gather.3
